TPU v7x, 32 devices: a whole 2x2x4 slice. The times are simulated.
32 devices in a mesh: sp: 8 (over z, y), tp: 4 (over x, core).
Axes of the slice: x: 2, y: 2, z: 4, core: 2. Of those that a mesh axis runs over, the one named last changes fastest.
Arguments:
- hidden: bfloat16 [6144, 2048], P(('sp', 'tp')), may hold values from -6 to 6
- norm_gain: float32 [2, 2048], replicated, may hold values from 0.1 to 1.9
- w_value: bfloat16 [2, 2048, 2048], P(None, 'sp', 'tp'), may hold values from -0.125 to 0.125
- w_gate: bfloat16 [2, 2048, 2048], P(None, 'sp', 'tp'), may hold values from -0.125 to 0.125
- conv_weight: float32 [2, 31, 2048], P(None, None, 'tp'), may hold values from -3 to 3
- conv_bias: float32 [2, 2048], P(None, 'tp'), may hold values from -3 to 3
- chan_gain: float32 [2, 2048], P(None, 'tp'), may hold values from 0.1 to 1.9
- chan_shift: float32 [2, 2048], P(None, 'tp'), may hold values from -3 to 3
- w_out: bfloat16 [2, 2048, 2048], P(None, 'tp', 'sp'), may hold values from -0.125 to 0.125
Outputs:
- result: bfloat16 [6144, 2048], P(('sp', 'tp'))
All inputs are finite; a program needn't handle non-finite values.
Results may differ from a plain program's by a relative error of at most 0.015.
Values may be sent and summed in bfloat16 or wider, within the bound.
A program may use at most 64 MiB of HBM per device.

v0:
```python
import jax
import jax.numpy as jnp
from jax import lax
from jax.sharding import PartitionSpec as P

EPS = 1e-06


def shifted(shard, axis, by):
    size = lax.axis_size(axis)
    pairs = [(i, i + by) for i in range(size) if 0 <= i + by < size]
    return lax.ppermute(shard, axis, pairs)


def body(hidden, norm_gain, w_value, w_gate, conv_weight, conv_bias, chan_gain, chan_shift, w_out):
    group = lax.axis_size("tp")
    own_rows = hidden.shape[0]
    chans = w_value.shape[2]
    taps = conv_weight.shape[1]
    state = hidden
    for layer in range(norm_gain.shape[0]):
        xf = state.astype(jnp.float32)
        scale = lax.rsqrt(jnp.mean(xf * xf, axis=1, keepdims=True) + EPS)
        normed = (xf * scale * norm_gain[layer][None, :]).astype(jnp.bfloat16)
        tokens = lax.all_gather(normed, "tp", axis=0, tiled=True)
        empty = jnp.zeros((tokens.shape[0], chans), jnp.float32)

        def add_both(totals, pieces, start, tokens=tokens):
            return (
                jnp.dot(tokens, pieces[0], preferred_element_type=jnp.float32),
                jnp.dot(tokens, pieces[1], preferred_element_type=jnp.float32),
            )

        lin, gate = add_both(
            (empty, empty),
            (
                lax.all_gather(w_value[layer], "sp", axis=0, tiled=True),
                lax.all_gather(w_gate[layer], "sp", axis=0, tiled=True),
            ),
            jnp.int32(0),
        )
        glu = (lin * jax.nn.sigmoid(gate)).astype(jnp.bfloat16)
        before = shifted(glu[tokens.shape[0] - (taps - 1) :], "sp", 1)
        window = jnp.concatenate([before, glu], axis=0).astype(jnp.float32)
        length = tokens.shape[0]
        mixed = jnp.zeros((length, chans), jnp.float32) + conv_bias[layer][None, :]
        for tap in range(taps):
            mixed = mixed + conv_weight[layer, tap][None, :] * window[tap : tap + length]
        totals = lax.psum((jnp.sum(mixed, axis=1), jnp.sum(mixed * mixed, axis=1)), "tp")
        mean = (totals[0] / (chans * group))[:, None]
        msq = (totals[1] / (chans * group))[:, None]
        var = msq - mean * mean
        act = jax.nn.silu(
            (mixed - mean) * lax.rsqrt(var + EPS) * chan_gain[layer][None, :]
            + chan_shift[layer][None, :]
        ).astype(jnp.bfloat16)

        def project(piece, start, act=act):
            return jnp.dot(act, piece, preferred_element_type=jnp.float32)

        partial_out = project(lax.all_gather(w_out[layer], "sp", axis=1, tiled=True), jnp.int32(0))

        def take_rows(start, count, partial_out=partial_out):
            return partial_out

        update = lax.psum_scatter(
            take_rows(jnp.int32(0), own_rows * lax.axis_size("tp")).astype(jnp.bfloat16),
            "tp",
            scatter_dimension=0,
            tiled=True,
        ).astype(jnp.float32)
        state = (xf + update).astype(jnp.bfloat16)
    return state


def solution(mesh):
    placed = (
        P(("sp", "tp"), None),
        P(),
        P(None, "sp", "tp"),
        P(None, "sp", "tp"),
        P(None, None, "tp"),
        P(None, "tp"),
        P(None, "tp"),
        P(None, "tp"),
        P(None, "tp", "sp"),
    )
    return jax.shard_map(
        body, mesh=mesh, in_specs=placed, out_specs=P(("sp", "tp"), None), check_vma=False
    )
```

profile of v0, /device:TPU:0, one launch (start us, length us, event | category | flops | bytes accessed | tf_op | source)
XLA Modules:
  0.0 466.3 jit_solution(699687578448124518)
XLA Ops:
  6.5 2.0 fusion.101
  8.5 0.0 all-gather.15.cloned.1.call-start
  8.6 0.2 fusion.10
  8.9 1.1 fusion.12
  10.0 0.0 all-gather.15.cloned.1.call-update
  10.1 0.0 all-gather.19.cloned.1.call-start
  10.1 0.8 fusion.100
  11.0 0.0 all-gather.19.cloned.1.call-update
  11.0 0.0 all-gather.23.cloned.1.call-start
  11.1 0.8 fusion.102
  11.9 0.0 reduce-scatter.3.cloned.1.call-start
  12.1 49.2 %all-gather.21.cloned.1.call-done = bf16[1,2048,512]{2,1,0:T(8,128)(2,1)} async-done(((bf16[1,256,512]{2,1,0:T(8,128)(2,1)}), bf16[1,2048,512]{2,1,0:T(8,128)(2,1)}) %all-gather.21.cloned.1.call-update) | async-done | bytes 2097168 | tf_op jit(solution)/shard_map/all_gather | solution.py:38
  61.3 28.6 %all-gather.15.cloned.1.call-done = bf16[768,2048]{1,0:T(8,128)(2,1)} async-done(((bf16[192,2048]{1,0:T(8,128)(2,1)}), bf16[768,2048]{1,0:T(8,128)(2,1)}) %all-gather.15.cloned.1.call-update) | async-done | bytes 3145744 | tf_op jit(solution)/shard_map/all_gather | solution.py:25
  89.9 4.3 fusion.6
  94.3 46.9 %all-gather.19.cloned.1.call-done = bf16[1,2048,512]{2,1,0:T(8,128)(2,1)} async-done(((bf16[1,256,512]{2,1,0:T(8,128)(2,1)}), bf16[1,2048,512]{2,1,0:T(8,128)(2,1)}) %all-gather.19.cloned.1.call-update) | async-done | bytes 2097168 | tf_op jit(solution)/shard_map/all_gather | solution.py:37
  141.2 4.5 multiply_convert_fusion.3
  145.7 2.5 collective-permute-start
  148.2 1.6 collective-permute-done
  149.7 0.2 maximum_convert_fusion
  150.0 6.9 %fusion.97 = (f32[768]{0:T(1024)S(1)}, f32[768]{0:T(1024)S(1)}, f32[768,512]{1,0:T(8,128)S(1)}) fusion(f32[798,512]{1,0:T(8,128)S(1)} %maximum_convert_fusion, f32[512]{0:T(512)S(1)} %bitcast.128, f32[512]{0:T(512)S(1)} %bitcast.129, f32[512]{0:T(512)S(1)} %bitcast.130, f32[512]{0:T(512)S(1)} %bitcast.131, f32[512]{0:T(512)S(1)} %bitcast.132, ...), kind=kLoop, calls=%fused_computation.177 | loop fusion | flops 25557504 | bytes 50403328 | tf_op jit(solution)/shard_map/reduce_sum | solution.py:49
  156.9 6.2 %all-reduce.1 = (f32[768]{0:T(1024)S(1)}, f32[768]{0:T(1024)S(1)}) all-reduce(f32[768]{0:T(1024)S(1)} %get-tuple-element.8, f32[768]{0:T(1024)S(1)} %get-tuple-element.7), channel_id=1, replica_groups=mesh['sp'=8,'tp'=4] {'tp'}, use_global_device_ids=true, to_apply=%region_4.0 | all-reduce | flops 1536 | bytes 12288 | tf_op jit(solution)/shard_map/psum | solution.py:49
  163.1 28.9 %all-gather.23.cloned.1.call-done = bf16[1,512,2048]{2,1,0:T(8,128)(2,1)} async-done(((bf16[1,512,256]{2,1,0:T(8,128)(2,1)}), bf16[1,512,2048]{2,1,0:T(8,128)(2,1)}) %all-gather.23.cloned.1.call-update) | async-done | bytes 2097168 | tf_op jit(solution)/shard_map/all_gather | solution.py:61
  192.0 5.3 %convolution_convert_fusion.1 = bf16[768,2048]{1,0:T(8,128)(2,1)} fusion(bf16[1,512,2048]{2,1,0:T(8,128)(2,1)} %all-gather.23.cloned.1.call-done, f32[768,512]{1,0:T(8,128)S(1)} %get-tuple-element.14, f32[512]{0:T(512)S(1)} %bitcast.165, f32[512]{0:T(512)S(1)} %bitcast.164, f32[768]{0:T(1024)S(1)} %get-tuple-element.94, f32[768]{0:T(1024)S(1)} %get-tuple-element.93), kind=kOutput, calls=%fused_computation.1 | convolution fusion | flops 1615724544 | bytes 6825984 | tf_op jit(solution)/shard_map/dot_general | solution.py:59
  197.4 0.0 all-gather.27.cloned.1.call-start
  197.4 0.5 all-gather.27.cloned.1.call-update
  197.9 0.0 all-gather.17.cloned.1.call-start
  198.0 35.6 %reduce-scatter.3.cloned.1.call-done = bf16[192,2048]{1,0:T(8,128)(2,1)} async-done(((bf16[768,2048]{1,0:T(8,128)(2,1)}), bf16[192,2048]{1,0:T(8,128)(2,1)}) %reduce-scatter.3.cloned.1.call-update) | async-done | bytes 786448 | tf_op jit(solution)/shard_map/reduce_scatter | solution.py:66
  233.5 1.5 fusion.14
  235.1 1.2 fusion.16
  236.4 0.0 all-gather.25.cloned.1.call-start
  236.4 0.7 all-gather.25.cloned.1.call-update
  237.1 0.0 all-gather.29.cloned.1.call-start
  237.2 0.7 all-gather.29.cloned.1.call-update
  237.8 0.0 reduce-scatter.5.cloned.1.call-start
  237.9 46.8 %all-gather.27.cloned.1.call-done = bf16[1,2048,512]{2,1,0:T(8,128)(2,1)} async-done(((bf16[1,256,512]{2,1,0:T(8,128)(2,1)}), bf16[1,2048,512]{2,1,0:T(8,128)(2,1)}) %all-gather.27.cloned.1.call-update) | async-done | bytes 2097168 | tf_op jit(solution)/shard_map/all_gather | solution.py:38
  284.7 28.6 %all-gather.17.cloned.1.call-done = bf16[768,2048]{1,0:T(8,128)(2,1)} async-done(((bf16[192,2048]{1,0:T(8,128)(2,1)}), bf16[768,2048]{1,0:T(8,128)(2,1)}) %all-gather.17.cloned.1.call-update) | async-done | bytes 3145744 | tf_op jit(solution)/shard_map/all_gather | solution.py:25
  313.3 4.3 fusion.1
  317.6 46.9 %all-gather.25.cloned.1.call-done = bf16[1,2048,512]{2,1,0:T(8,128)(2,1)} async-done(((bf16[1,256,512]{2,1,0:T(8,128)(2,1)}), bf16[1,2048,512]{2,1,0:T(8,128)(2,1)}) %all-gather.25.cloned.1.call-update) | async-done | bytes 2097168 | tf_op jit(solution)/shard_map/all_gather | solution.py:37
  364.5 4.5 multiply_convert_fusion.1
  369.0 2.7 collective-permute-start.1
  371.7 1.3 collective-permute-done.1
  373.1 0.2 maximum_convert_fusion.1
  373.3 6.9 %fusion.96 = (f32[768]{0:T(1024)S(1)}, f32[768]{0:T(1024)S(1)}, f32[768,512]{1,0:T(8,128)S(1)}) fusion(f32[798,512]{1,0:T(8,128)S(1)} %maximum_convert_fusion.1, f32[512]{0:T(512)S(1)} %bitcast.109, f32[512]{0:T(512)S(1)} %bitcast.98, f32[512]{0:T(512)S(1)} %bitcast.142, f32[512]{0:T(512)S(1)} %bitcast.143, f32[512]{0:T(512)S(1)} %bitcast.144, ...), kind=kLoop, calls=%fused_computation.176 | loop fusion | flops 25557504 | bytes 50403328 | tf_op jit(solution)/shard_map/reduce_sum | solution.py:49
  380.2 6.2 %all-reduce = (f32[768]{0:T(1024)S(1)}, f32[768]{0:T(1024)S(1)}) all-reduce(f32[768]{0:T(1024)S(1)} %get-tuple-element.6, f32[768]{0:T(1024)S(1)} %get-tuple-element.5), channel_id=1, replica_groups=mesh['sp'=8,'tp'=4] {'tp'}, use_global_device_ids=true, to_apply=%region_10.11 | all-reduce | flops 1536 | bytes 12288 | tf_op jit(solution)/shard_map/psum | solution.py:49
  386.4 29.1 %all-gather.29.cloned.1.call-done = bf16[1,512,2048]{2,1,0:T(8,128)(2,1)} async-done(((bf16[1,512,256]{2,1,0:T(8,128)(2,1)}), bf16[1,512,2048]{2,1,0:T(8,128)(2,1)}) %all-gather.29.cloned.1.call-update) | async-done | bytes 2097168 | tf_op jit(solution)/shard_map/all_gather | solution.py:61
  415.5 5.3 %convolution_convert_fusion = bf16[768,2048]{1,0:T(8,128)(2,1)} fusion(bf16[1,512,2048]{2,1,0:T(8,128)(2,1)} %all-gather.29.cloned.1.call-done, f32[768,512]{1,0:T(8,128)S(1)} %get-tuple-element.13, f32[512]{0:T(512)S(1)} %bitcast.163, f32[512]{0:T(512)S(1)} %bitcast.162, f32[768]{0:T(1024)S(1)} %get-tuple-element.86, f32[768]{0:T(1024)S(1)} %get-tuple-element.85), kind=kOutput, calls=%fused_computation | convolution fusion | flops 1615724544 | bytes 6825984 | tf_op jit(solution)/shard_map/dot_general | solution.py:59
  420.9 36.2 %reduce-scatter.5.cloned.1.call-done = bf16[192,2048]{1,0:T(8,128)(2,1)} async-done(((bf16[768,2048]{1,0:T(8,128)(2,1)}), bf16[192,2048]{1,0:T(8,128)(2,1)}) %reduce-scatter.5.cloned.1.call-update) | async-done | bytes 786448 | tf_op jit(solution)/shard_map/reduce_scatter | solution.py:66
  457.1 2.4 fusion.17
  (38 shorter events, 0.4 us)
Async XLA Ops:
  6.5 2.1 copy-start
  6.5 2.3 copy-start.5
  6.5 54.8 %all-gather.21.cloned.1.call-start = ((), (), s32[]{:S(2)}) async-start(), calls=%async_computation.7 | async-start | bytes 2359296 | tf_op jit(solution)/shard_map/all_gather | solution.py:38
  8.5 1.6 copy-start.2
  8.5 81.4 %all-gather.15.cloned.1.call-start = ((), (), s32[]{:S(2)}) async-start(), calls=%async_computation.2 | async-start | bytes 3932160 | tf_op jit(solution)/shard_map/all_gather | solution.py:25
  8.9 2.2 copy-start.3
  10.0 2.0 copy-start.4
  10.0 2.0 copy-start.6
  10.1 2.1 copy-start.7
  10.1 131.1 %all-gather.19.cloned.1.call-start = ((), (), s32[]{:S(2)}) async-start(), calls=%async_computation.6 | async-start | bytes 2359296 | tf_op jit(solution)/shard_map/all_gather | solution.py:37
  11.0 181.0 %all-gather.23.cloned.1.call-start = ((), (), s32[]{:S(2)}) async-start(), calls=%async_computation.8 | async-start | bytes 2359296 | tf_op jit(solution)/shard_map/all_gather | solution.py:61
  11.9 221.6 %reduce-scatter.3.cloned.1.call-start = ((), (), s32[]{:S(2)}) async-start(), calls=%async_computation.3 | async-start | bytes 3932160 | tf_op jit(solution)/shard_map/reduce_scatter | solution.py:66
  94.3 53.9 %copy-start.8 = (f32[2,512]{1,0:T(2,128)S(1)}, f32[2,512]{1,0:T(2,128)}, u32[]{:S(2)}) copy-start(f32[2,512]{1,0:T(2,128)} %param.16) | copy-start | bytes 12292
  145.7 4.0 collective-permute-start
  197.4 87.3 %all-gather.27.cloned.1.call-start = ((), (), s32[]{:S(2)}) async-start(), calls=%async_computation.10 | async-start | bytes 2359296 | tf_op jit(solution)/shard_map/all_gather | solution.py:38
  197.9 115.4 %all-gather.17.cloned.1.call-start = ((), (), s32[]{:S(2)}) async-start(), calls=%async_computation.4 | async-start | bytes 3932160 | tf_op jit(solution)/shard_map/all_gather | solution.py:25
  233.5 1.6 copy-start.1
  236.4 128.2 %all-gather.25.cloned.1.call-start = ((), (), s32[]{:S(2)}) async-start(), calls=%async_computation.9 | async-start | bytes 2359296 | tf_op jit(solution)/shard_map/all_gather | solution.py:37
  237.1 178.4 %all-gather.29.cloned.1.call-start = ((), (), s32[]{:S(2)}) async-start(), calls=%async_computation.11 | async-start | bytes 2359296 | tf_op jit(solution)/shard_map/all_gather | solution.py:61
  237.8 219.2 %reduce-scatter.5.cloned.1.call-start = ((), (), s32[]{:S(2)}) async-start(), calls=%async_computation.5 | async-start | bytes 3932160 | tf_op jit(solution)/shard_map/reduce_scatter | solution.py:66
  369.0 4.1 collective-permute-start.1
Sparse Core Ops, SparseCore 0:
  9.5 51.7 all-gather.20
  62.9 27.0 all-gather.14
  92.1 49.0 all-gather.18
  143.1 48.8 all-gather.22
  197.5 36.0 reduce-scatter.2
  235.5 49.0 all-gather.26
  286.2 27.0 all-gather.16
  315.4 49.0 all-gather.24
  366.6 48.8 all-gather.28
  421.0 36.0 reduce-scatter.4
where the time goes:
time: 467 us; the launch traced here: 466 us
  waiting for transfers between devices  382 us (82%)
  matrix products  28.3 us (6%)
  other arithmetic  20.8 us (4%)
  between operations  13.8 us (3%)
  blocking collectives  12.3 us (3%)
  starting transfers between devices  5.48 us (1%)
    all_gather x2, waiting for transfers between devices, body(): lax.all_gather(w_gate[layer], 'sp', axis=0, tiled=True)  95.9 us
    all_gather x2, waiting for transfers between devices, body(): lax.all_gather(w_value[layer], 'sp', axis=0, tiled=True)  93.8 us
    reduce_scatter x2, waiting for transfers between devices, body(): lax.psum_scatter(take_rows(jnp.int32(0), own_rows * lax.axis_size('tp'))....  71.8 us
    all_gather x2, waiting for transfers between devices, body(): lax.all_gather(w_out[layer], 'sp', axis=1, tiled=True)  58 us
    all_gather x2, waiting for transfers between devices, body(): tokens = lax.all_gather(normed, 'tp', axis=0, tiled=True)  57.3 us
    reduce_sum x2, other arithmetic, body(): jnp.sum(mixed, axis=1)  13.8 us
    psum x2, blocking collectives, body(): lax.psum((jnp.sum(mixed, axis=1), jnp.sum(mixed * mixed, axis=1)), 'tp')  12.3 us
    dot_general x2, matrix products, project(): return jnp.dot(act, piece, preferred_element_type=jnp.float32)  10.7 us
  transfers between devices with their start and end apart: 12, of which 12 were waited for; matrix products, arithmetic and copies ran while one was open for 8% of the time, Pallas kernels for 0%

commit v1 on v0

--- a/solution.py
+++ b/solution.py
@@ -22,7 +22,14 @@
         xf = state.astype(jnp.float32)
         scale = lax.rsqrt(jnp.mean(xf * xf, axis=1, keepdims=True) + EPS)
         normed = (xf * scale * norm_gain[layer][None, :]).astype(jnp.bfloat16)
-        tokens = lax.all_gather(normed, "tp", axis=0, tiled=True)
+        ring = [normed]
+        for hop in range(3):
+            ring.append(lax.ppermute(ring[-1], "tp", [(dev, (dev + 1) % 4) for dev in range(4)]))
+        tokens = jnp.roll(
+            jnp.concatenate(ring[::-1], axis=0),
+            (lax.axis_index("tp") + 1) * ring[0].shape[0],
+            axis=0,
+        )
         empty = jnp.zeros((tokens.shape[0], chans), jnp.float32)
 
         def add_both(totals, pieces, start, tokens=tokens):

time: 467 us -> 406 us (0.87)
  waiting for transfers between devices: 382 us -> 291 us
  other arithmetic: 20.8 us -> 49.8 us
    all_gather x2, waiting for transfers between devices: 95.9 us -> 0.34 us  [body(): lax.all_gather(w_gate[layer], 'sp', axis=0, tiled=True)]
    ppermute x0 -> x6, waiting for transfers between devices: none -> 67 us  [body(): lax.ppermute(ring[-1], 'tp', [(dev, (dev + 1) % 4) for dev in range(4)])]
    all_gather x2 -> x0, waiting for transfers between devices: 57.3 us -> none  [body(): tokens = lax.all_gather(normed, 'tp', axis=0, tiled=True)]
    concatenate x0 -> x2, other arithmetic: none -> 30.7 us  [body(): jnp.roll(jnp.concatenate(ring[::-1], axis=0), (lax.axis_index('tp') + 1)...]
  transfers between devices with their start and end apart: 12 -> 16, of which waited for: 12 -> 15; matrix products, arithmetic and copies ran while one was open for 8% -> 17% of each run, Pallas kernels for 0% -> 0%
where the time goes in v1:
time: 406 us
  waiting for transfers between devices  291 us (72%)
  other arithmetic  49.8 us (12%)
  matrix products  28.2 us (7%)
  between operations  13.8 us (3%)
  blocking collectives  12.3 us (3%)
  starting transfers between devices  6 us (1%)
  local copies, waits for them, and re-layouts  4.86 us (1%)
    all_gather x2, waiting for transfers between devices, body(): lax.all_gather(w_value[layer], 'sp', axis=0, tiled=True)  90.3 us
    reduce_scatter x2, waiting for transfers between devices, body(): lax.psum_scatter(take_rows(jnp.int32(0), own_rows * lax.axis_size('tp'))....  71.2 us
    ppermute x6, waiting for transfers between devices, body(): lax.ppermute(ring[-1], 'tp', [(dev, (dev + 1) % 4) for dev in range(4)])  67 us
    all_gather x2, waiting for transfers between devices, body(): lax.all_gather(w_out[layer], 'sp', axis=1, tiled=True)  58.1 us
    concatenate x2, other arithmetic, body(): jnp.roll(jnp.concatenate(ring[::-1], axis=0), (lax.axis_index('tp') + 1)...  30.7 us
    reduce_sum x2, other arithmetic, body(): jnp.sum(mixed, axis=1)  13.8 us
    psum x2, blocking collectives, body(): lax.psum((jnp.sum(mixed, axis=1), jnp.sum(mixed * mixed, axis=1)), 'tp')  12.3 us
    dot_general x2, matrix products, project(): return jnp.dot(act, piece, preferred_element_type=jnp.float32)  10.6 us
  transfers between devices with their start and end apart: 16, of which 15 were waited for; matrix products, arithmetic and copies ran while one was open for 17% of the time, Pallas kernels for 0%

profile of v1, /device:TPU:0, one launch (start us, length us, event | category | flops | bytes accessed | tf_op | source)
XLA Modules:
  0.0 406.1 jit_solution(9651381716040389489)
XLA Ops:
  6.5 2.0 fusion.115
  8.5 0.0 all-gather.13.cloned.1.call-start
  8.6 0.8 fusion.114
  9.4 0.0 all-gather.17.cloned.1.call-start
  9.5 0.2 fusion.24
  9.8 0.3 fusion.26
  10.1 0.5 collective-permute-start
  10.6 11.6 %collective-permute-done = bf16[192,2048]{1,0:T(8,128)(2,1)S(1)} collective-permute-done((bf16[192,2048]{1,0:T(8,128)(2,1)S(1)}, bf16[192,2048]{1,0:T(8,128)(2,1)S(1)}, u32[]{:S(2)}, u32[]{:S(2)}) %collective-permute-start) | collective-permute-done | bytes 786464 | tf_op jit(solution)/shard_map/ppermute | solution.py:27
  22.2 1.8 fusion.116
  24.1 0.0 reduce-scatter.3.cloned.1.call-start
  24.1 9.5 %collective-permute-done.1 = bf16[192,2048]{1,0:T(8,128)(2,1)S(1)} collective-permute-done((bf16[192,2048]{1,0:T(8,128)(2,1)S(1)}, bf16[192,2048]{1,0:T(8,128)(2,1)S(1)}, u32[]{:S(2)}, u32[]{:S(2)}) %collective-permute-start.1) | collective-permute-done | bytes 786464 | tf_op jit(solution)/shard_map/ppermute | solution.py:27
  33.8 11.4 %collective-permute-done.2 = bf16[192,2048]{1,0:T(8,128)(2,1)} collective-permute-done((bf16[192,2048]{1,0:T(8,128)(2,1)S(1)}, bf16[192,2048]{1,0:T(8,128)(2,1)}, u32[]{:S(2)}, u32[]{:S(2)}) %collective-permute-start.2) | collective-permute-done | bytes 786464 | tf_op jit(solution)/shard_map/ppermute | solution.py:27
  45.1 15.8 %fusion.10 = bf16[768,2048]{1,0:T(8,128)(2,1)} fusion(s32[]{:T(128)S(6)} %select_n.13, bf16[192,2048]{1,0:T(8,128)(2,1)} %collective-permute-done.2, bf16[192,2048]{1,0:T(8,128)(2,1)S(1)} %collective-permute-done.1, bf16[192,2048]{1,0:T(8,128)(2,1)S(1)} %collective-permute-done, bf16[192,2048]{1,0:T(8,128)(2,1)S(1)} %fusion.26), kind=kLoop, calls=%fused_computation.28 | loop fusion | flops 25165824 | bytes 6291460 | tf_op jit(solution)/shard_map/jit(_roll_dynamic)/concatenate | solution.py:28
  61.0 0.3 all-gather.15.cloned.1.call-done
  61.3 4.3 %fusion.20 = f32[768,512]{1,0:T(8,128)S(1)} fusion(bf16[768,2048]{1,0:T(8,128)(2,1)} %fusion.10, bf16[1,2048,512]{2,1,0:T(8,128)(2,1)} %all-gather.15.cloned.1.call-done), kind=kOutput, calls=%fused_computation.44 | convolution fusion | flops 1610612736 | bytes 6815744 | tf_op jit(solution)/shard_map/dot_general | solution.py:38
  65.6 45.4 %all-gather.13.cloned.1.call-done = bf16[1,2048,512]{2,1,0:T(8,128)(2,1)} async-done(((bf16[1,256,512]{2,1,0:T(8,128)(2,1)}), bf16[1,2048,512]{2,1,0:T(8,128)(2,1)}) %all-gather.13.cloned.1.call-update) | async-done | bytes 2097168 | tf_op jit(solution)/shard_map/all_gather | solution.py:44
  111.1 4.5 %multiply_convert_fusion.3 = bf16[768,512]{1,0:T(8,128)(2,1)S(1)} fusion(f32[768,512]{1,0:T(8,128)S(1)} %fusion.20, bf16[768,2048]{1,0:T(8,128)(2,1)} %fusion.10, bf16[1,2048,512]{2,1,0:T(8,128)(2,1)} %all-gather.13.cloned.1.call-done), kind=kOutput, calls=%fused_computation.185 | convolution fusion | flops 1612578816 | bytes 7602176 | tf_op jit(solution)/shard_map/dot_general | solution.py:37
  115.6 2.6 collective-permute-start.3
  118.3 1.4 collective-permute-done.3
  119.6 0.2 maximum_convert_fusion
  119.9 6.9 %fusion.111 = (f32[768]{0:T(1024)S(1)}, f32[768]{0:T(1024)S(1)}, f32[768,512]{1,0:T(8,128)S(1)}) fusion(f32[798,512]{1,0:T(8,128)S(1)} %maximum_convert_fusion, f32[512]{0:T(512)S(1)} %bitcast.132, f32[512]{0:T(512)S(1)} %bitcast.133, f32[512]{0:T(512)S(1)} %bitcast.134, f32[512]{0:T(512)S(1)} %bitcast.135, f32[512]{0:T(512)S(1)} %bitcast.136, ...), kind=kLoop, calls=%fused_computation.207 | loop fusion | flops 25557504 | bytes 50403328 | tf_op jit(solution)/shard_map/reduce_sum | solution.py:56
  126.8 6.2 %all-reduce.1 = (f32[768]{0:T(1024)S(1)}, f32[768]{0:T(1024)S(1)}) all-reduce(f32[768]{0:T(1024)S(1)} %get-tuple-element.9, f32[768]{0:T(1024)S(1)} %get-tuple-element.8), channel_id=1, replica_groups=mesh['sp'=8,'tp'=4] {'tp'}, use_global_device_ids=true, to_apply=%region_4.6 | all-reduce | flops 1536 | bytes 12288 | tf_op jit(solution)/shard_map/psum | solution.py:56
  133.0 29.1 %all-gather.17.cloned.1.call-done = bf16[1,512,2048]{2,1,0:T(8,128)(2,1)} async-done(((bf16[1,512,256]{2,1,0:T(8,128)(2,1)}), bf16[1,512,2048]{2,1,0:T(8,128)(2,1)}) %all-gather.17.cloned.1.call-update) | async-done | bytes 2097168 | tf_op jit(solution)/shard_map/all_gather | solution.py:68
  162.0 5.3 %convolution_convert_fusion.1 = bf16[768,2048]{1,0:T(8,128)(2,1)} fusion(bf16[1,512,2048]{2,1,0:T(8,128)(2,1)} %all-gather.17.cloned.1.call-done, f32[768,512]{1,0:T(8,128)S(1)} %get-tuple-element.15, f32[512]{0:T(512)S(1)} %bitcast.165, f32[512]{0:T(512)S(1)} %bitcast.164, f32[768]{0:T(1024)S(1)} %get-tuple-element.95, f32[768]{0:T(1024)S(1)} %get-tuple-element.94), kind=kOutput, calls=%fused_computation.17 | convolution fusion | flops 1615724544 | bytes 6825984 | tf_op jit(solution)/shard_map/dot_general | solution.py:66
  167.4 0.0 all-gather.21.cloned.1.call-start
  167.4 0.5 all-gather.21.cloned.1.call-update
  168.0 0.5 all-gather.19.cloned.1.call-update
  168.6 35.0 %reduce-scatter.3.cloned.1.call-done = bf16[192,2048]{1,0:T(8,128)(2,1)} async-done(((bf16[768,2048]{1,0:T(8,128)(2,1)}), bf16[192,2048]{1,0:T(8,128)(2,1)}) %reduce-scatter.3.cloned.1.call-update) | async-done | bytes 786448 | tf_op jit(solution)/shard_map/reduce_scatter | solution.py:73
  203.6 1.5 fusion.28
  205.2 0.3 fusion.30
  205.5 0.1 collective-permute-start.4
  205.6 11.4 %collective-permute-done.4 = bf16[192,2048]{1,0:T(8,128)(2,1)S(1)} collective-permute-done((bf16[192,2048]{1,0:T(8,128)(2,1)S(1)}, bf16[192,2048]{1,0:T(8,128)(2,1)S(1)}, u32[]{:S(2)}, u32[]{:S(2)}) %collective-permute-start.4) | collective-permute-done | bytes 786464 | tf_op jit(solution)/shard_map/ppermute | solution.py:27
  217.0 11.5 %collective-permute-done.5 = bf16[192,2048]{1,0:T(8,128)(2,1)} collective-permute-done((bf16[192,2048]{1,0:T(8,128)(2,1)S(1)}, bf16[192,2048]{1,0:T(8,128)(2,1)}, u32[]{:S(2)}, u32[]{:S(2)}) %collective-permute-start.5) | collective-permute-done | bytes 786464 | tf_op jit(solution)/shard_map/ppermute | solution.py:27
  228.5 0.0 reduce-scatter.5.cloned.1.call-start
  228.6 11.7 %collective-permute-done.6 = bf16[192,2048]{1,0:T(8,128)(2,1)} collective-permute-done((bf16[192,2048]{1,0:T(8,128)(2,1)}, bf16[192,2048]{1,0:T(8,128)(2,1)}, u32[]{:S(2)}, u32[]{:S(2)}) %collective-permute-start.6) | collective-permute-done | bytes 786464 | tf_op jit(solution)/shard_map/ppermute | solution.py:27
  240.2 14.9 %fusion.3 = bf16[768,2048]{1,0:T(8,128)(2,1)} fusion(s32[]{:T(128)S(6)} %select_n.13, bf16[192,2048]{1,0:T(8,128)(2,1)} %collective-permute-done.6, bf16[192,2048]{1,0:T(8,128)(2,1)} %collective-permute-done.5, bf16[192,2048]{1,0:T(8,128)(2,1)S(1)} %collective-permute-done.4, bf16[192,2048]{1,0:T(8,128)(2,1)S(1)} %fusion.30), kind=kLoop, calls=%fused_computation.21 | loop fusion | flops 25165824 | bytes 6291460 | tf_op jit(solution)/shard_map/jit(_roll_dynamic)/concatenate | solution.py:28
  255.1 4.3 %fusion.15 = f32[768,512]{1,0:T(8,128)S(1)} fusion(bf16[768,2048]{1,0:T(8,128)(2,1)} %fusion.3, bf16[1,2048,512]{2,1,0:T(8,128)(2,1)} %all-gather.21.cloned.1.call-done), kind=kOutput, calls=%fused_computation.39 | convolution fusion | flops 1610612736 | bytes 6815744 | tf_op jit(solution)/shard_map/dot_general | solution.py:38
  259.5 44.9 %all-gather.19.cloned.1.call-done = bf16[1,2048,512]{2,1,0:T(8,128)(2,1)} async-done(((bf16[1,256,512]{2,1,0:T(8,128)(2,1)}), bf16[1,2048,512]{2,1,0:T(8,128)(2,1)}) %all-gather.19.cloned.1.call-update) | async-done | bytes 2097168 | tf_op jit(solution)/shard_map/all_gather | solution.py:44
  304.4 4.5 %multiply_convert_fusion.1 = bf16[768,512]{1,0:T(8,128)(2,1)S(1)} fusion(f32[768,512]{1,0:T(8,128)S(1)} %fusion.15, bf16[768,2048]{1,0:T(8,128)(2,1)} %fusion.3, bf16[1,2048,512]{2,1,0:T(8,128)(2,1)} %all-gather.19.cloned.1.call-done), kind=kOutput, calls=%fused_computation.182 | convolution fusion | flops 1612578816 | bytes 7602176 | tf_op jit(solution)/shard_map/dot_general | solution.py:37
  308.8 2.5 collective-permute-start.7
  311.4 1.5 collective-permute-done.7
  312.9 0.2 maximum_convert_fusion.1
  313.1 6.9 %fusion.110 = (f32[768]{0:T(1024)S(1)}, f32[768]{0:T(1024)S(1)}, f32[768,512]{1,0:T(8,128)S(1)}) fusion(f32[798,512]{1,0:T(8,128)S(1)} %maximum_convert_fusion.1, f32[512]{0:T(512)S(1)} %bitcast.98, f32[512]{0:T(512)S(1)} %bitcast.99, f32[512]{0:T(512)S(1)} %bitcast.142, f32[512]{0:T(512)S(1)} %bitcast.143, f32[512]{0:T(512)S(1)} %bitcast.144, ...), kind=kLoop, calls=%fused_computation.206 | loop fusion | flops 25557504 | bytes 50403328 | tf_op jit(solution)/shard_map/reduce_sum | solution.py:56
  320.0 6.2 %all-reduce = (f32[768]{0:T(1024)S(1)}, f32[768]{0:T(1024)S(1)}) all-reduce(f32[768]{0:T(1024)S(1)} %get-tuple-element.7, f32[768]{0:T(1024)S(1)} %get-tuple-element.6), channel_id=1, replica_groups=mesh['sp'=8,'tp'=4] {'tp'}, use_global_device_ids=true, to_apply=%region_10.12 | all-reduce | flops 1536 | bytes 12288 | tf_op jit(solution)/shard_map/psum | solution.py:56
  326.2 29.1 %all-gather.23.cloned.1.call-done = bf16[1,512,2048]{2,1,0:T(8,128)(2,1)} async-done(((bf16[1,512,256]{2,1,0:T(8,128)(2,1)}), bf16[1,512,2048]{2,1,0:T(8,128)(2,1)}) %all-gather.23.cloned.1.call-update) | async-done | bytes 2097168 | tf_op jit(solution)/shard_map/all_gather | solution.py:68
  355.3 5.3 %convolution_convert_fusion = bf16[768,2048]{1,0:T(8,128)(2,1)} fusion(bf16[1,512,2048]{2,1,0:T(8,128)(2,1)} %all-gather.23.cloned.1.call-done, f32[768,512]{1,0:T(8,128)S(1)} %get-tuple-element.14, f32[512]{0:T(512)S(1)} %bitcast.163, f32[512]{0:T(512)S(1)} %bitcast.162, f32[768]{0:T(1024)S(1)} %get-tuple-element.87, f32[768]{0:T(1024)S(1)} %get-tuple-element.86), kind=kOutput, calls=%fused_computation.16 | convolution fusion | flops 1615724544 | bytes 6825984 | tf_op jit(solution)/shard_map/dot_general | solution.py:66
  360.6 36.2 %reduce-scatter.5.cloned.1.call-done = bf16[192,2048]{1,0:T(8,128)(2,1)} async-done(((bf16[768,2048]{1,0:T(8,128)(2,1)}), bf16[192,2048]{1,0:T(8,128)(2,1)}) %reduce-scatter.5.cloned.1.call-update) | async-done | bytes 786448 | tf_op jit(solution)/shard_map/reduce_scatter | solution.py:73
  396.8 2.4 fusion.31
  (44 shorter events, 0.4 us)
Async XLA Ops:
  6.5 2.0 copy-start.2
  6.5 3.0 copy-start
  6.5 3.2 copy-start.4
  6.5 54.8 %all-gather.15.cloned.1.call-start = ((), (), s32[]{:S(2)}) async-start(), calls=%async_computation.5 | async-start | bytes 2359296 | tf_op jit(solution)/shard_map/all_gather | solution.py:45
  8.5 102.6 %all-gather.13.cloned.1.call-start = ((), (), s32[]{:S(2)}) async-start(), calls=%async_computation.4 | async-start | bytes 2359296 | tf_op jit(solution)/shard_map/all_gather | solution.py:44
  9.4 152.6 %all-gather.17.cloned.1.call-start = ((), (), s32[]{:S(2)}) async-start(), calls=%async_computation.6 | async-start | bytes 2359296 | tf_op jit(solution)/shard_map/all_gather | solution.py:68
  9.7 14.4 %copy-start.5 = (f32[2,512]{1,0:T(2,128)S(1)}, f32[2,512]{1,0:T(2,128)}, u32[]{:S(2)}) copy-start(f32[2,512]{1,0:T(2,128)} %param.16) | copy-start | bytes 12292
  9.7 23.9 %copy-start.6 = (f32[2,512]{1,0:T(2,128)S(1)}, f32[2,512]{1,0:T(2,128)}, u32[]{:S(2)}) copy-start(f32[2,512]{1,0:T(2,128)} %param.17) | copy-start | bytes 12292
  9.8 23.9 %copy-start.3 = (f32[2,31,512]{2,0,1:T(2,128)S(1)}, f32[2,31,512]{2,0,1:T(2,128)}, u32[]{:S(2)}) copy-start(f32[2,31,512]{2,0,1:T(2,128)} %param.15) | copy-start | bytes 380932
  10.1 12.1 %collective-permute-start = (bf16[192,2048]{1,0:T(8,128)(2,1)S(1)}, bf16[192,2048]{1,0:T(8,128)(2,1)S(1)}, u32[]{:S(2)}, u32[]{:S(2)}) collective-permute-start(bf16[192,2048]{1,0:T(8,128)(2,1)S(1)} %fusion.26), channel_id=1, source_target_pairs={{0,1},{1,2},{2,3},{3,0},{4,5},{5,6},{6,7},{7,4},{8,9},{9,10},{10,1... | collective-permute-start | bytes 2359304 | tf_op jit(solution)/shard_map/ppermute | solution.py:27
  22.2 11.4 %collective-permute-start.1 = (bf16[192,2048]{1,0:T(8,128)(2,1)S(1)}, bf16[192,2048]{1,0:T(8,128)(2,1)S(1)}, u32[]{:S(2)}, u32[]{:S(2)}) collective-permute-start(bf16[192,2048]{1,0:T(8,128)(2,1)S(1)} %collective-permute-done), channel_id=1, source_target_pairs={{0,1},{1,2},{2,3},{3,0},{4,5},{5,6},{6,7},{7,4},{8,9},{9,10},{10,1... | collective-permute-start | bytes 2359304 | tf_op jit(solution)/shard_map/ppermute | solution.py:27
  24.1 179.5 %reduce-scatter.3.cloned.1.call-start = ((), (), s32[]{:S(2)}) async-start(), calls=%async_computation.2 | async-start | bytes 3932160 | tf_op jit(solution)/shard_map/reduce_scatter | solution.py:73
  33.6 11.5 %collective-permute-start.2 = (bf16[192,2048]{1,0:T(8,128)(2,1)S(1)}, bf16[192,2048]{1,0:T(8,128)(2,1)}, u32[]{:S(2)}, u32[]{:S(2)}) collective-permute-start(bf16[192,2048]{1,0:T(8,128)(2,1)S(1)} %collective-permute-done.1), channel_id=1, source_target_pairs={{0,1},{1,2},{2,3},{3,0},{4,5},{5,6},{6,7},{7,4},{8,9},{9,10},{10,1... | collective-permute-start | bytes 2359304 | tf_op jit(solution)/shard_map/ppermute | solution.py:27
  65.6 52.6 %copy-start.7 = (f32[2,512]{1,0:T(2,128)S(1)}, f32[2,512]{1,0:T(2,128)}, u32[]{:S(2)}) copy-start(f32[2,512]{1,0:T(2,128)} %param.18) | copy-start | bytes 12292
  115.6 4.1 collective-permute-start.3
  167.4 87.7 %all-gather.21.cloned.1.call-start = ((), (), s32[]{:S(2)}) async-start(), calls=%async_computation.8 | async-start | bytes 2359296 | tf_op jit(solution)/shard_map/all_gather | solution.py:45
  168.0 136.4 %all-gather.19.cloned.1.call-start = ((), (), s32[]{:S(2)}) async-start(), calls=%async_computation.7 | async-start | bytes 2359296 | tf_op jit(solution)/shard_map/all_gather | solution.py:44
  168.6 186.7 %all-gather.23.cloned.1.call-start = ((), (), s32[]{:S(2)}) async-start(), calls=%async_computation.9 | async-start | bytes 2359296 | tf_op jit(solution)/shard_map/all_gather | solution.py:68
  203.6 1.6 copy-start.1
  205.5 11.5 %collective-permute-start.4 = (bf16[192,2048]{1,0:T(8,128)(2,1)S(1)}, bf16[192,2048]{1,0:T(8,128)(2,1)S(1)}, u32[]{:S(2)}, u32[]{:S(2)}) collective-permute-start(bf16[192,2048]{1,0:T(8,128)(2,1)S(1)} %fusion.30), channel_id=1, source_target_pairs={{0,1},{1,2},{2,3},{3,0},{4,5},{5,6},{6,7},{7,4},{8,9},{9,10},{10,1... | collective-permute-start | bytes 2359304 | tf_op jit(solution)/shard_map/ppermute | solution.py:27
  217.0 11.5 %collective-permute-start.5 = (bf16[192,2048]{1,0:T(8,128)(2,1)S(1)}, bf16[192,2048]{1,0:T(8,128)(2,1)}, u32[]{:S(2)}, u32[]{:S(2)}) collective-permute-start(bf16[192,2048]{1,0:T(8,128)(2,1)S(1)} %collective-permute-done.4), channel_id=1, source_target_pairs={{0,1},{1,2},{2,3},{3,0},{4,5},{5,6},{6,7},{7,4},{8,9},{9,10},{10,1... | collective-permute-start | bytes 2359304 | tf_op jit(solution)/shard_map/ppermute | solution.py:27
  228.5 11.7 %collective-permute-start.6 = (bf16[192,2048]{1,0:T(8,128)(2,1)}, bf16[192,2048]{1,0:T(8,128)(2,1)}, u32[]{:S(2)}, u32[]{:S(2)}) collective-permute-start(bf16[192,2048]{1,0:T(8,128)(2,1)} %collective-permute-done.5), channel_id=1, source_target_pairs={{0,1},{1,2},{2,3},{3,0},{4,5},{5,6},{6,7},{7,4},{8,9},{9,10},{10,1... | collective-permute-start | bytes 2359304 | tf_op jit(solution)/shard_map/ppermute | solution.py:27
  228.5 168.3 %reduce-scatter.5.cloned.1.call-start = ((), (), s32[]{:S(2)}) async-start(), calls=%async_computation.3 | async-start | bytes 3932160 | tf_op jit(solution)/shard_map/reduce_scatter | solution.py:73
  308.8 4.0 collective-permute-start.7
Sparse Core Ops, SparseCore 0:
  9.5 51.7 all-gather.14
  63.4 47.6 all-gather.12
  113.1 48.8 all-gather.16
  167.5 36.0 reduce-scatter.2
  205.6 49.0 all-gather.20
  256.7 47.6 all-gather.18
  306.4 48.8 all-gather.22
  360.8 36.0 reduce-scatter.4
